TPU v7x, 32 devices: a whole 2x2x4 slice. The times are simulated.
32 devices in a mesh: sp: 16 (over z, y, x), tp: 2 (over core).
Axes of the slice: x: 2, y: 2, z: 4, core: 2. Of those that a mesh axis runs over, the one named last changes fastest.
Arguments:
- value_in: bfloat16 [4096, 2048], P('sp', 'tp'), may hold values from -25 to 25, as said below
- gate_in: bfloat16 [4096, 2048], P('sp', 'tp'), may hold values from -6 to 6
- taps: float32 [31, 2048], P(None, 'tp'), may hold values from -1 to 1
- gain: float32 [2048], P('tp'), may hold values from 0.1 to 1.9
- shift: float32 [2048], P('tp'), may hold values from -3 to 3
- w_out: bfloat16 [2048, 2048], P('tp'), may hold values from -0.125 to 0.125
- grad_out: bfloat16 [4096, 2048], P('sp'), may hold values from -6 to 6
Outputs:
- d_value: bfloat16 [4096, 2048], P('sp', 'tp')
- d_gate: bfloat16 [4096, 2048], P('sp', 'tp')
- d_taps: float32 [31, 2048], P(None, 'tp')
- d_gain: float32 [2048], P('tp')
- d_shift: float32 [2048], P('tp')
Inputs may be any that keep to these rules, and one draw needn't show every extreme that they name: `value_in`: channel blocks of different magnitude.
All inputs are finite; a program needn't handle non-finite values.
Results may differ from a plain program's by a relative error of at most 0.007.
Values may be sent and summed in bfloat16 or wider, within the bound.
A program may use at most 64 MiB of HBM per device.

v0:
```python
import math

import jax
import jax.numpy as jnp
from jax import lax
from jax.sharding import PartitionSpec as P

EPS = 1e-05


def with_halo(block, sides, width):
    for axis, dim in sides:
        count = lax.axis_size(axis)
        forward = [(i, i + 1) for i in range(count - 1)]
        backward = [(target, source) for source, target in forward]
        low = lax.ppermute(
            lax.slice_in_dim(block, block.shape[dim] - width, None, axis=dim), axis, forward
        )
        high = lax.ppermute(lax.slice_in_dim(block, 0, width, axis=dim), axis, backward)
        block = jnp.concatenate([low, block, high], axis=dim)
    return block


def gated_rows(value_rows, gate_rows):
    gate_sig = jax.nn.sigmoid(gate_rows.astype(jnp.float32))
    return ((value_rows.astype(jnp.float32) * gate_sig).astype(jnp.bfloat16), gate_sig)


def convolve(window, taps, count):
    wide = window.astype(jnp.float32)
    total = jnp.zeros((count, wide.shape[1]), jnp.float32)
    for offset in range(taps.shape[0]):
        total = total + taps[offset] * wide[offset : offset + count]
    return total


def norm_backward(conv_out, grad_rows, gain, shift, w_out, width):
    sums, squares = lax.psum((jnp.sum(conv_out, 1), jnp.sum(conv_out * conv_out, 1)), "tp")
    mean = sums / width
    var = squares / width - mean * mean
    inv = lax.rsqrt(var + EPS)
    normed = (conv_out - mean[:, None]) * inv[:, None]
    pre = normed * gain + shift
    grad_mix = lax.dot_general(
        grad_rows, w_out, (((1,), (1,)), ((), ())), preferred_element_type=jnp.float32
    )
    sig = jax.nn.sigmoid(pre)
    grad_pre = grad_mix * sig * (1.0 + pre * (1.0 - sig))
    grad_normed = grad_pre * gain
    first, second = lax.psum((jnp.sum(grad_normed, 1), jnp.sum(grad_normed * normed, 1)), "tp")
    grad_conv = inv[:, None] * (
        grad_normed - first[:, None] / width - normed * second[:, None] / width
    )
    return (grad_conv, grad_pre, normed)


def shards(value_in, gate_in, taps, gain, shift, w_out, grad_out):
    half = taps.shape[0] // 2
    kernel = taps.shape[0]
    rows = value_in.shape[0]
    width = value_in.shape[1] * lax.axis_size("tp")
    total = rows * lax.axis_size("sp")
    gated, gate_sig = gated_rows(value_in, gate_in)
    gated_wide = with_halo(gated, (("sp", 0),), half)
    conv_out = convolve(gated_wide, taps, rows)
    grad_conv, grad_pre, normed = norm_backward(conv_out, grad_out, gain, shift, w_out, width)
    grad_wide = with_halo(grad_conv, (("sp", 0),), half)
    own_grad = grad_wide[half : half + rows]
    gated_float = gated_wide.astype(jnp.float32)
    grad_gated = jnp.zeros((rows, own_grad.shape[1]), jnp.float32)
    for offset in range(kernel):
        grad_gated = (
            grad_gated + taps[offset] * grad_wide[2 * half - offset : 2 * half - offset + rows]
        )
    tap_terms = jnp.stack(
        [jnp.sum(own_grad * gated_float[offset : offset + rows], 0) for offset in range(kernel)]
    )
    scale = 1.0 / math.sqrt(total)
    stacked = (
        jnp.concatenate(
            [tap_terms, jnp.sum(grad_pre * normed, 0)[None], jnp.sum(grad_pre, 0)[None]], 0
        )
        * scale
    )
    summed = lax.psum(stacked, "sp")
    d_taps = summed[:kernel]
    d_gain = summed[kernel]
    d_shift = summed[kernel + 1]
    d_value = (grad_gated * gate_sig).astype(jnp.bfloat16)
    d_gate = (grad_gated * value_in.astype(jnp.float32) * gate_sig * (1.0 - gate_sig)).astype(
        jnp.bfloat16
    )
    return (d_value, d_gate, d_taps, d_gain, d_shift)


def solution(mesh):
    return jax.shard_map(
        shards,
        mesh=mesh,
        in_specs=(
            P("sp", "tp"),
            P("sp", "tp"),
            P(None, "tp"),
            P("tp"),
            P("tp"),
            P("tp", None),
            P("sp", None),
        ),
        out_specs=(P("sp", "tp"), P("sp", "tp"), P(None, "tp"), P("tp"), P("tp")),
        check_vma=False,
    )
```

profile of v0, /device:TPU:0, one launch (start us, length us, event | category | flops | bytes accessed | tf_op | source)
XLA Modules:
  0.0 175.2 jit_solution(298959568165321427)
XLA Ops:
  7.2 0.0 copy-start
  7.2 0.0 all-reduce.4.cloned.1.call-start
  7.2 1.6 fusion.1
  8.9 4.9 %collective-permute-start = (bf16[15,1024]{1,0:T(8,128)(2,1)S(1)}, bf16[15,1024]{1,0:T(8,128)(2,1)S(1)}, u32[]{:S(2)}, u32[]{:S(2)}) collective-permute-start(bf16[15,1024]{1,0:T(8,128)(2,1)S(1)} %get-tuple-element.52), channel_id=1, source_target_pairs={{0,2},{2,4},{4,6},{6,8},{8,10},{10,12},{12,14},{14,16},{16,18},{18... | collective-permute-start | bytes 92168 | tf_op jit(solution)/shard_map/ppermute | solution.py:16
  13.7 1.3 collective-permute-start.1
  15.0 0.1 fusion.97
  15.2 0.0 copy-start.12
  15.2 0.0 copy-start.13
  15.3 0.0 collective-permute-done
  15.4 4.2 %collective-permute-done.1 = bf16[15,1024]{1,0:T(8,128)(2,1)S(1)} collective-permute-done((bf16[15,1024]{1,0:T(8,128)(2,1)S(1)}, bf16[15,1024]{1,0:T(8,128)(2,1)S(1)}, u32[]{:S(2)}, u32[]{:S(2)}) %collective-permute-start.1) | collective-permute-done | bytes 30752 | tf_op jit(solution)/shard_map/ppermute | solution.py:19
  19.5 0.2 maximum_convert_fusion
  19.7 0.0 copy-start.24
  19.7 0.0 copy-start.25
  19.7 5.7 %multiply_reduce_fusion.33 = (f32[256]{0:T(256)S(1)}, f32[256]{0:T(256)S(1)}, f32[256,1024]{1,0:T(8,128)S(1)}) fusion(f32[286,1024]{1,0:T(8,128)S(1)} %maximum_convert_fusion, f32[1024]{0:T(1024)S(1)} %bitcast.126, f32[1024]{0:T(1024)S(1)} %bitcast.128, f32[1024]{0:T(1024)S(1)} %bitcast.70, f32[1024]{0:T(1024)S(1)} %bitcast.72, f32[1024]{0:T(1024)S(1)} %bitcast.74, ...), kind=kLoop, calls=%fused_computation.186 | loop fusion | flops 16776704 | bytes 33683456 | tf_op jit(solution)/shard_map/reduce_sum | solution.py:38
  25.6 2.5 %all-reduce.1 = (f32[256]{0:T(256)S(1)}, f32[256]{0:T(256)S(1)}) all-reduce(f32[256]{0:T(256)S(1)} %get-tuple-element.41, f32[256]{0:T(256)S(1)} %get-tuple-element.40), channel_id=1, replica_groups=mesh['sp'=16,'tp'=2] {'tp'}, use_global_device_ids=true, to_apply=%region_3.0 | all-reduce | flops 512 | bytes 4096 | tf_op jit(solution)/shard_map/psum | solution.py:38
  28.1 5.5 %multiply_reduce_fusion = (f32[1024]{0:T(1024)}, f32[256]{0:T(256)S(1)}, f32[256]{0:T(256)S(1)}, f32[1024]{0:T(1024)}, f32[256,1024]{1,0:T(8,128)}) fusion(f32[256,1024]{1,0:T(8,128)S(1)} %get-tuple-element.49, f32[256]{0:T(256)S(1)} %get-tuple-element.88, f32[256]{0:T(256)S(1)} %get-tuple-element.87, f32[1024]{0:T(1024)S(1)} %copy-done.24, ...), kind=kOutput, calls=%fused_computation.150 | convolution fusion | flops 1078720000 | bytes 7360512 | tf_op jit(solution)/shard_map/dot_general | solution.py:44
  33.7 2.4 %all-reduce = (f32[256]{0:T(256)S(1)}, f32[256]{0:T(256)S(1)}) all-reduce(f32[256]{0:T(256)S(1)} %get-tuple-element.37, f32[256]{0:T(256)S(1)} %get-tuple-element.38), channel_id=1, replica_groups=mesh['sp'=16,'tp'=2] {'tp'}, use_global_device_ids=true, to_apply=%region_7.0 | all-reduce | flops 512 | bytes 4096 | tf_op jit(solution)/shard_map/psum | solution.py:50
  36.1 4.8 %multiply_reduce_fusion.1 = (f32[1024]{0:T(1024)}, f32[1024]{0:T(1024)}, f32[1024]{0:T(1024)}, f32[1024]{0:T(1024)}, f32[1024]{0:T(1024)}, /*index=5*/f32[1024]{...) fusion(f32[286,1024]{1,0:T(8,128)S(1)} %maximum_convert_fusion,, ...), kind=kLoop, calls=%fused_computation.151 | loop fusion | flops 11515904 | bytes 22102016 | tf_op jit(solution)/shard_map/reduce_sum | solution.py:76
  41.0 2.4 %multiply_reduce_fusion.2 = (f32[1024]{0:T(1024)}, f32[1024]{0:T(1024)}, f32[1024]{0:T(1024)}, f32[1024]{0:T(1024)}, f32[1024]{0:T(1024)}, /*index=5*/f32[1024]{...) fusion(f32[256,1024]{1,0:T(8,128)S(1)} %get-tuple-element.46, ...), kind=kLoop, calls=%fused_computation.152 | loop fusion | flops 6802432 | bytes 14733312 | tf_op jit(solution)/shard_map/reduce_sum | solution.py:76
  43.3 0.6 fusion.94
  44.0 1.3 collective-permute-start.2
  45.3 4.9 %collective-permute-start.3 = (f32[15,1024]{1,0:T(8,128)S(1)}, f32[15,1024]{1,0:T(8,128)S(1)}, u32[]{:S(2)}, u32[]{:S(2)}) collective-permute-start(f32[15,1024]{1,0:T(8,128)S(1)} %get-tuple-element.51), channel_id=1, source_target_pairs={{0,2},{2,4},{4,6},{6,8},{8,10},{10,12},{12,14},{14,16},{16,18},{18... | collective-permute-start | bytes 184328 | tf_op jit(solution)/shard_map/ppermute | solution.py:16
  50.2 3.8 %concatenate.44 = f32[33,1024]{1,0:T(8,128)S(1)} concatenate(f32[1,1024]{1,0:T(1,128)} %bitcast.160, f32[1,1024]{1,0:T(1,128)} %bitcast.159, f32[1,1024]{1,0:T(1,128)} %bitcast.158, f32[1,1024]{1,0:T(1,128)} %bitcast.157, f32[1,1024]{1,0:T(1,128)} %bitcast.156, f32[1,1024]{1,0:T(1,128)} %bitcast.155, f32[1,1024]{1,0:T(1,128)} %bitcast.154, f32[1,1024]{1,0:T(1,128)} %bitcast.153, ...), dimensions={0} | concatenate | bytes 270336 | tf_op jit(solution)/shard_map/concatenate | solution.py:80
  54.0 0.7 broadcast_multiply_fusion
  54.7 0.0 all-reduce.4.cloned.1.call-update
  54.7 0.0 collective-permute-done.2
  54.7 0.0 collective-permute-done.3
  54.8 6.9 %fusion.4 = (bf16[256,1024]{1,0:T(8,128)(2,1)}, f32[256,1024]{1,0:T(8,128)}) fusion(bf16[256,1024]{1,0:T(8,128)(2,1)S(1)} %copy-done.3, bf16[256,1024]{1,0:T(8,128)(2,1)S(1)} %copy-done.1, f32[256,1024]{1,0:T(8,128)S(1)} %get-tuple-element.46, f32[15,1024]{1,0:T(8,128)S(1)} %collective-permute-done.3, f32[1024]{0:T(1024)} %bitcast.127, f32[1024]{0:T(1024)} %bitcast.129, ...), kind=kLoop, calls=%fused_computation.35 | loop fusion | flops 26476544 | bytes 3919872 | tf_op jit(solution)/shard_map/convert_element_type | solution.py:90
  61.7 2.3 %multiply_convert_fusion = bf16[256,1024]{1,0:T(8,128)(2,1)} fusion(f32[256,1024]{1,0:T(8,128)} %get-tuple-element.48, bf16[256,1024]{1,0:T(8,128)(2,1)S(1)} %copy-done.1), kind=kLoop, calls=%fused_computation.182 | loop fusion | flops 1572864 | bytes 2097152 | tf_op jit(solution)/shard_map/convert_element_type | solution.py:89
  64.0 101.4 %all-reduce.4.cloned.1.call-done = f32[33,1024]{1,0:T(8,128)} async-done(((f32[33,1024]{1,0:T(8,128)}), f32[33,1024]{1,0:T(8,128)}) %all-reduce.4.cloned.1.call-update) | async-done | bytes 135184 | tf_op jit(solution)/shard_map/psum | solution.py:85
  165.4 1.4 fusion.96
  166.8 1.6 slice.579
  (51 shorter events, 0.2 us)
Async XLA Ops:
  7.2 20.9 %copy-start = (bf16[256,2048]{1,0:T(8,128)(2,1)S(1)}, bf16[256,2048]{1,0:T(8,128)(2,1)}, u32[]{:S(2)}) copy-start(bf16[256,2048]{1,0:T(8,128)(2,1)} %param.13) | copy-start | bytes 3145732
  7.2 7.9 %copy-start.4 = (f32[31,1024]{1,0:T(8,128)S(1)}, f32[31,1024]{1,0:T(8,128)}, u32[]{:S(2)}) copy-start(f32[31,1024]{1,0:T(8,128)} %param.9) | copy-start | bytes 380932
  7.2 158.2 %all-reduce.4.cloned.1.call-start = ((), (), s32[]{:S(2)}) async-start(), calls=%async_computation | async-start | bytes 327680 | tf_op jit(solution)/shard_map/psum | solution.py:85
  8.9 6.5 %collective-permute-start = (bf16[15,1024]{1,0:T(8,128)(2,1)S(1)}, bf16[15,1024]{1,0:T(8,128)(2,1)S(1)}, u32[]{:S(2)}, u32[]{:S(2)}) collective-permute-start(bf16[15,1024]{1,0:T(8,128)(2,1)S(1)} %get-tuple-element.52), channel_id=1, source_target_pairs={{0,2},{2,4},{4,6},{6,8},{8,10},{10,12},{12,14},{14,16},{16,18},{18... | collective-permute-start | bytes 92168 | tf_op jit(solution)/shard_map/ppermute | solution.py:16
  13.7 5.8 %collective-permute-start.1 = (bf16[15,1024]{1,0:T(8,128)(2,1)S(1)}, bf16[15,1024]{1,0:T(8,128)(2,1)S(1)}, u32[]{:S(2)}, u32[]{:S(2)}) collective-permute-start(bf16[15,1024]{1,0:T(8,128)(2,1)S(1)} %get-tuple-element.53), channel_id=1, source_target_pairs={{2,0},{4,2},{6,4},{8,6},{10,8},{12,10},{14,12},{16,14},{18,16},{20... | collective-permute-start | bytes 92168 | tf_op jit(solution)/shard_map/ppermute | solution.py:19
  15.1 10.3 %copy-start.5 = (f32[1,1024]{1,0:T(1,128)}, f32[1,1024]{1,0:T(1,128)S(1)}, u32[]{:S(2)}) copy-start(f32[1,1024]{1,0:T(1,128)S(1)} %get-tuple-element.68) | copy-start | bytes 12292
  15.1 10.3 %copy-start.6 = (f32[1,1024]{1,0:T(1,128)}, f32[1,1024]{1,0:T(1,128)S(1)}, u32[]{:S(2)}) copy-start(f32[1,1024]{1,0:T(1,128)S(1)} %get-tuple-element.69) | copy-start | bytes 12292
  15.1 10.3 %copy-start.7 = (f32[1,1024]{1,0:T(1,128)}, f32[1,1024]{1,0:T(1,128)S(1)}, u32[]{:S(2)}) copy-start(f32[1,1024]{1,0:T(1,128)S(1)} %get-tuple-element.70) | copy-start | bytes 12292
  15.1 10.3 %copy-start.8 = (f32[1,1024]{1,0:T(1,128)}, f32[1,1024]{1,0:T(1,128)S(1)}, u32[]{:S(2)}) copy-start(f32[1,1024]{1,0:T(1,128)S(1)} %get-tuple-element.71) | copy-start | bytes 12292
  15.1 10.3 %copy-start.9 = (f32[1,1024]{1,0:T(1,128)}, f32[1,1024]{1,0:T(1,128)S(1)}, u32[]{:S(2)}) copy-start(f32[1,1024]{1,0:T(1,128)S(1)} %get-tuple-element.72) | copy-start | bytes 12292
  15.2 10.3 %copy-start.10 = (f32[1,1024]{1,0:T(1,128)}, f32[1,1024]{1,0:T(1,128)S(1)}, u32[]{:S(2)}) copy-start(f32[1,1024]{1,0:T(1,128)S(1)} %get-tuple-element.73) | copy-start | bytes 12292
  15.2 10.3 %copy-start.11 = (f32[1,1024]{1,0:T(1,128)}, f32[1,1024]{1,0:T(1,128)S(1)}, u32[]{:S(2)}) copy-start(f32[1,1024]{1,0:T(1,128)S(1)} %get-tuple-element.74) | copy-start | bytes 12292
  15.2 10.3 %copy-start.12 = (f32[1,1024]{1,0:T(1,128)}, f32[1,1024]{1,0:T(1,128)S(1)}, u32[]{:S(2)}) copy-start(f32[1,1024]{1,0:T(1,128)S(1)} %get-tuple-element.75) | copy-start | bytes 12292
  15.2 10.3 %copy-start.13 = (f32[1,1024]{1,0:T(1,128)}, f32[1,1024]{1,0:T(1,128)S(1)}, u32[]{:S(2)}) copy-start(f32[1,1024]{1,0:T(1,128)S(1)} %get-tuple-element.76) | copy-start | bytes 12292
  15.2 10.3 %copy-start.14 = (f32[1,1024]{1,0:T(1,128)}, f32[1,1024]{1,0:T(1,128)S(1)}, u32[]{:S(2)}) copy-start(f32[1,1024]{1,0:T(1,128)S(1)} %get-tuple-element.77) | copy-start | bytes 12292
  15.3 10.3 %copy-start.15 = (f32[1,1024]{1,0:T(1,128)}, f32[1,1024]{1,0:T(1,128)S(1)}, u32[]{:S(2)}) copy-start(f32[1,1024]{1,0:T(1,128)S(1)} %get-tuple-element.78) | copy-start | bytes 12292
  15.3 10.3 %copy-start.16 = (f32[1,1024]{1,0:T(1,128)}, f32[1,1024]{1,0:T(1,128)S(1)}, u32[]{:S(2)}) copy-start(f32[1,1024]{1,0:T(1,128)S(1)} %get-tuple-element.79) | copy-start | bytes 12292
  15.3 10.3 %copy-start.17 = (f32[1,1024]{1,0:T(1,128)}, f32[1,1024]{1,0:T(1,128)S(1)}, u32[]{:S(2)}) copy-start(f32[1,1024]{1,0:T(1,128)S(1)} %get-tuple-element.80) | copy-start | bytes 12292
  15.3 10.3 %copy-start.18 = (f32[1,1024]{1,0:T(1,128)}, f32[1,1024]{1,0:T(1,128)S(1)}, u32[]{:S(2)}) copy-start(f32[1,1024]{1,0:T(1,128)S(1)} %get-tuple-element.81) | copy-start | bytes 12292
  15.3 10.3 %copy-start.19 = (f32[1,1024]{1,0:T(1,128)}, f32[1,1024]{1,0:T(1,128)S(1)}, u32[]{:S(2)}) copy-start(f32[1,1024]{1,0:T(1,128)S(1)} %get-tuple-element.82) | copy-start | bytes 12292
  15.3 10.3 %copy-start.20 = (f32[1,1024]{1,0:T(1,128)}, f32[1,1024]{1,0:T(1,128)S(1)}, u32[]{:S(2)}) copy-start(f32[1,1024]{1,0:T(1,128)S(1)} %get-tuple-element.83) | copy-start | bytes 12292
  15.3 10.3 %copy-start.21 = (f32[1,1024]{1,0:T(1,128)}, f32[1,1024]{1,0:T(1,128)S(1)}, u32[]{:S(2)}) copy-start(f32[1,1024]{1,0:T(1,128)S(1)} %get-tuple-element.84) | copy-start | bytes 12292
  15.3 10.3 %copy-start.22 = (f32[1,1024]{1,0:T(1,128)}, f32[1,1024]{1,0:T(1,128)S(1)}, u32[]{:S(2)}) copy-start(f32[1,1024]{1,0:T(1,128)S(1)} %get-tuple-element.85) | copy-start | bytes 12292
  15.3 10.3 %copy-start.23 = (f32[1,1024]{1,0:T(1,128)}, f32[1,1024]{1,0:T(1,128)S(1)}, u32[]{:S(2)}) copy-start(f32[1,1024]{1,0:T(1,128)S(1)} %get-tuple-element.86) | copy-start | bytes 12292
  19.7 8.4 %copy-start.24 = (f32[1024]{0:T(1024)S(1)}, f32[1024]{0:T(1024)}, u32[]{:S(2)}) copy-start(f32[1024]{0:T(1024)} %param.10) | copy-start | bytes 12292
  19.7 8.4 %copy-start.25 = (f32[1024]{0:T(1024)S(1)}, f32[1024]{0:T(1024)}, u32[]{:S(2)}) copy-start(f32[1024]{0:T(1024)} %param.11) | copy-start | bytes 12292
  25.6 8.0 %copy-start.2 = (f32[256,1024]{1,0:T(8,128)}, f32[256,1024]{1,0:T(8,128)S(1)}, u32[]{:S(2)}) copy-start(f32[256,1024]{1,0:T(8,128)S(1)} %get-tuple-element.49) | copy-start | bytes 3145732
  43.3 11.4 %copy-start.1 = (bf16[256,1024]{1,0:T(8,128)(2,1)S(1)}, bf16[256,1024]{1,0:T(8,128)(2,1)}, u32[]{:S(2)}) copy-start(bf16[256,1024]{1,0:T(8,128)(2,1)} %param.8) | copy-start | bytes 1572868
  43.3 11.4 %copy-start.3 = (bf16[256,1024]{1,0:T(8,128)(2,1)S(1)}, bf16[256,1024]{1,0:T(8,128)(2,1)}, u32[]{:S(2)}) copy-start(bf16[256,1024]{1,0:T(8,128)(2,1)} %param.7) | copy-start | bytes 1572868
  44.0 10.7 %collective-permute-start.2 = (f32[15,1024]{1,0:T(8,128)}, f32[15,1024]{1,0:T(8,128)S(1)}, u32[]{:S(2)}, u32[]{:S(2)}) collective-permute-start(f32[15,1024]{1,0:T(8,128)} %get-tuple-element.50), channel_id=1, source_target_pairs={{2,0},{4,2},{6,4},{8,6},{10,8},{12,10},{14,12},{16,14},{18,16},{20... | collective-permute-start | bytes 184328 | tf_op jit(solution)/shard_map/ppermute | solution.py:19
  45.3 9.5 %collective-permute-start.3 = (f32[15,1024]{1,0:T(8,128)S(1)}, f32[15,1024]{1,0:T(8,128)S(1)}, u32[]{:S(2)}, u32[]{:S(2)}) collective-permute-start(f32[15,1024]{1,0:T(8,128)S(1)} %get-tuple-element.51), channel_id=1, source_target_pairs={{0,2},{2,4},{4,6},{6,8},{8,10},{10,12},{12,14},{14,16},{16,18},{18... | collective-permute-start | bytes 184328 | tf_op jit(solution)/shard_map/ppermute | solution.py:16
Sparse Core Ops, SparseCore 0:
  54.8 110.4 all-reduce.3
where the time goes:
time: 176 us; the launch traced here: 175 us
  waiting for transfers between devices  106 us (60%)
  other arithmetic  24.5 us (14%)
  between operations  14.5 us (8%)
  starting transfers between devices  12.4 us (7%)
  local copies, waits for them, and re-layouts  7.63 us (4%)
  matrix products  5.53 us (3%)
  blocking collectives  4.91 us (3%)
    psum x1, waiting for transfers between devices, shards(): summed = lax.psum(stacked, 'sp')  101 us
    ppermute x2, starting transfers between devices, with_halo(): lax.ppermute(lax.slice_in_dim(block, block.shape[dim] - width, None, axis...  9.8 us
    reduce_sum x2, other arithmetic, shards(): jnp.sum(own_grad * gated_float[offset:offset + rows], 0)  7.23 us
    convert_element_type x1, other arithmetic, shards(): (grad_gated * value_in.astype(jnp.float32) * gate_sig * (1.0 - gate_sig))...  6.89 us
    reduce_sum x1, other arithmetic, norm_backward(): jnp.sum(conv_out * conv_out, 1)  5.69 us
    dot_general x1, matrix products, norm_backward(): lax.dot_general(grad_rows, w_out, (((1,), (1,)), ((), ())), preferred_ele...  5.53 us
    ppermute x2, waiting for transfers between devices, with_halo(): lax.ppermute(lax.slice_in_dim(block, 0, width, axis=dim), axis, backward)  4.19 us
    concatenate x1, local copies, waits for them, and re-layouts, shards(): jnp.concatenate([tap_terms, jnp.sum(grad_pre * normed, 0)[None], jnp.sum(...  3.82 us
  transfers between devices with their start and end apart: 5, of which 2 were waited for; matrix products, arithmetic and copies ran while one was open for 8% of the time, Pallas kernels for 0%

commit v1 on v0

v1 whole, which is shorter than its diff:
```python
import functools
import math

import jax
import jax.numpy as jnp
import numpy as np
from jax import lax
from jax.experimental import pallas as pl
from jax.experimental.pallas import tpu as pltpu
from jax.sharding import PartitionSpec as P

EPS = 1e-05
ALIGN = 16
LANES = 128
CHUNK = 256
F32 = jnp.float32
BF16 = jnp.bfloat16


class Plan:
    def __init__(self, rows, kernel, total):
        self.half = kernel // 2
        self.kernel = kernel
        self.rows = rows
        self.edge = -(-(self.half + 1) // ALIGN) * ALIGN
        edge = self.edge
        self.size = rows // 2 + 4 * edge
        size = self.size
        self.freqs = size // 2
        self.wide = rows + 4 * edge
        self.mid = rows + 2 * edge
        self.fwd_out = self.mid // 2
        self.fwd_step = self.wide - size
        self.bwd_out = rows // 2
        self.bwd_step = self.mid - size
        omega = 2.0 * np.pi * (np.arange(self.freqs) + 0.5) / size

        def spectrum(times):
            angle = omega[:, None] * times[None, :]
            return np.concatenate([np.cos(angle), np.sin(angle)], 0)

        def inverse(times):
            angle = times[:, None] * omega[None, :]
            return np.concatenate([np.cos(angle), -np.sin(angle)], 1)

        forward = spectrum(np.arange(size))
        conv = []
        grad = []
        own = []
        for b in range(2):
            start = b * self.fwd_out + edge - self.half - b * self.fwd_step
            conv.append(inverse(np.arange(self.fwd_out) + start))
            start = b * self.bwd_out + edge + self.half - b * self.bwd_step
            grad.append(inverse(np.arange(self.bwd_out) + start))
            start = b * self.bwd_out + edge - b * self.bwd_step
            own.append(spectrum(np.arange(self.bwd_out) + start))
        self.tap_rows = -(-kernel // ALIGN) * ALIGN
        lags = inverse(np.arange(self.tap_rows) - self.half)
        lags[kernel:] = 0.0
        self.mats = np.concatenate([forward] + conv + grad + [lags], 0)
        self.at_conv = size
        self.at_grad = self.at_conv + self.mid
        self.at_lags = self.at_grad + rows
        self.own = np.concatenate(own, 0)
        self.taps = spectrum(np.arange(kernel)) * (2.0 / size)
        self.lag_scale = 2.0 / size / math.sqrt(total)


def dot(a, b):
    return jnp.dot(a, b, preferred_element_type=F32)


def sigmoid(x):
    return 0.5 * jnp.tanh(0.5 * x) + 0.5


def body(
    plan, n, tiles, per, total,
    value_h, gate_h, taps_h, gain_h, shift_h, w_h, go_h, mats_h, own_h, ft_h,
    dv_h, dg_h, dt_o, dgs_o,
    value, gate, taps, gain, shift, w, go, mats, own, ft,
    sig_s, gw, conv, gm, gcw, ts, hs, gs_spec, acc1, acc2,
    st1, st1_in, st2, st2_in, inv_s, colg, cols,
    gs, rs_src, rs_in, ag, dv, dg,
    load_sem, w_sem, out_sem, halo_send, halo_recv, tp_send, tp_recv,
    all_send, all_recv,
):
    sp = lax.axis_index("sp")
    tp = lax.axis_index("tp")
    rows, edge, half2 = plan.rows, plan.edge, 2 * plan.edge
    channels = value.shape[1]
    width = channels * 2
    chunks = channels // CHUNK
    size, freqs, mid = plan.size, plan.freqs, plan.mid
    nxt = lax.rem(sp + 1, n)
    prv = lax.rem(sp + n - 1, n)

    def peer(d):
        return lax.rem(sp + d, n)

    barrier = pltpu.get_barrier_semaphore()

    def greet(d, carry):
        pl.semaphore_signal(
            barrier, 1, device_id=(peer(d), tp), device_id_type=pl.DeviceIdType.MESH
        )
        return carry

    pl.semaphore_signal(
        barrier, 1, device_id=(sp, 1 - tp), device_id_type=pl.DeviceIdType.MESH
    )
    lax.fori_loop(1, n, greet, 0)

    own_go = go.at[pl.ds(edge, rows)]
    pairs = [
        (value_h, value), (gate_h, gate), (taps_h, taps), (ft_h, ft), (own_h, own),
        (mats_h, mats), (go_h, own_go), (gain_h, gain), (shift_h, shift),
    ]
    loads = [
        pltpu.make_async_copy(a, b, load_sem.at[i]) for i, (a, b) in enumerate(pairs)
    ]
    for load in loads:
        load.start()

    def w_copy(c):
        part = pl.ds(pl.multiple_of(c * CHUNK, CHUNK), CHUNK)
        return pltpu.make_async_copy(w_h.at[part], w.at[part], w_sem.at[c])

    for c in range(chunks):
        w_copy(c).start()

    def cut(c):
        return pl.ds(pl.multiple_of(c * CHUNK, CHUNK), CHUNK)

    loads[0].wait()
    loads[1].wait()

    def gate_step(i, carry):
        part = pl.ds(pl.multiple_of(i * ALIGN, ALIGN), ALIGN)
        place = pl.ds(pl.multiple_of(i * ALIGN + half2, ALIGN), ALIGN)
        sig = sigmoid(gate[part].astype(F32))
        sig_s[part] = sig
        gw[place] = (value[part].astype(F32) * sig).astype(BF16)
        return carry

    lax.fori_loop(0, rows // ALIGN, gate_step, 0)
    for load in loads[2:7]:
        load.wait()

    def tap_step(c, carry):
        ts[:, cut(c)] = jnp.dot(
            ft[...], taps[:, cut(c)], precision=lax.Precision.HIGHEST,
            preferred_element_type=F32,
        )
        return carry

    lax.fori_loop(0, chunks, tap_step, 0)

    pl.semaphore_wait(barrier, n)

    def remote(src, dst, send, recv, device):
        return pltpu.make_async_remote_copy(
            src_ref=src, dst_ref=dst, send_sem=send, recv_sem=recv,
            device_id=device, device_id_type=pl.DeviceIdType.MESH,
        )

    halos = [
        remote(gw.at[pl.ds(rows, half2)], gw.at[pl.ds(0, half2)],
               halo_send.at[0], halo_recv.at[0], (nxt, tp)),
        remote(gw.at[pl.ds(half2, half2)], gw.at[pl.ds(rows + half2, half2)],
               halo_send.at[1], halo_recv.at[1], (prv, tp)),
        remote(go.at[pl.ds(rows, edge)], go.at[pl.ds(0, edge)],
               halo_send.at[2], halo_recv.at[2], (nxt, tp)),
        remote(go.at[pl.ds(edge, edge)], go.at[pl.ds(rows + edge, edge)],
               halo_send.at[3], halo_recv.at[3], (prv, tp)),
    ]
    for halo in halos:
        halo.start()

    def mix(a, b):
        return lax.dot_general(a, b, (((1,), (1,)), ((), ())), preferred_element_type=F32)

    def own_step(c, carry):
        for b in range(2):
            hs[pl.ds(b * size, size), cut(c)] = dot(
                own[pl.ds(b * size, size)],
                gw[pl.ds(half2 + b * plan.bwd_out, plan.bwd_out), cut(c)],
            )
        return carry

    lax.fori_loop(0, chunks, own_step, 0)

    def mix_step(c, carry):
        w_copy(c).wait()
        gm[pl.ds(edge, rows), cut(c)] = mix(go[pl.ds(edge, rows)], w[cut(c)])
        return carry

    lax.fori_loop(0, chunks, mix_step, 0)

    halos[0].wait_recv()
    halos[1].wait_recv()

    @pl.when(sp == 0)
    def _():
        gw[pl.ds(0, half2)] = jnp.zeros((half2, channels), BF16)

    @pl.when(sp == n - 1)
    def _():
        gw[pl.ds(rows + half2, half2)] = jnp.zeros((half2, channels), BF16)

    acc1[...] = jnp.zeros_like(acc1)
    acc2[...] = jnp.zeros_like(acc2)

    def fold(x):
        out = x[:, :LANES]
        for k in range(1, x.shape[1] // LANES):
            out = out + x[:, k * LANES : (k + 1) * LANES]
        return out

    def conv_step(c, carry):
        ta = ts[pl.ds(0, freqs), cut(c)]
        tb = ts[pl.ds(freqs, freqs), cut(c)]
        for b in range(2):
            spec = dot(mats[pl.ds(0, size)], gw[pl.ds(b * plan.fwd_step, size), cut(c)])
            re, im = spec[:freqs], spec[freqs:]
            prod = jnp.concatenate([re * ta + im * tb, re * tb - im * ta], 0).astype(BF16)
            out = dot(mats[pl.ds(plan.at_conv + b * plan.fwd_out, plan.fwd_out)], prod)
            place = pl.ds(b * plan.fwd_out, plan.fwd_out)
            conv[place, cut(c)] = out
            acc1[place] += fold(out)
            acc2[place] += fold(out * out)
        return carry

    lax.fori_loop(0, chunks, conv_step, 0)

    first_lanes = lax.broadcasted_iota(jnp.int32, (mid, LANES), 1) < LANES // 2
    st1[...] = jnp.where(
        first_lanes,
        jnp.sum(acc1[...], 1, keepdims=True),
        jnp.sum(acc2[...], 1, keepdims=True),
    )
    swap1 = remote(st1, st1_in, tp_send.at[0], tp_recv.at[0], (sp, 1 - tp))
    swap1.start()

    halos[2].wait_recv()
    halos[3].wait_recv()

    def edge_step(c, carry):
        both = jnp.concatenate([go[pl.ds(0, edge)], go[pl.ds(rows + edge, edge)]], 0)
        out = mix(both, w[cut(c)])
        gm[pl.ds(0, edge), cut(c)] = out[:edge]
        gm[pl.ds(rows + edge, edge), cut(c)] = out[edge:]
        return carry

    lax.fori_loop(0, chunks, edge_step, 0)
    loads[7].wait()
    loads[8].wait()
    colg[...] = jnp.zeros_like(colg)
    cols[...] = jnp.zeros_like(cols)
    swap1.wait_recv()
    lanes = lax.broadcasted_iota(jnp.int32, (ALIGN, LANES), 1) < LANES // 2

    def norm_step(i, carry):
        part = pl.ds(pl.multiple_of(i * ALIGN, ALIGN), ALIGN)
        tot = (st1[part] + st1_in[part]) * (1.0 / width)
        mean = tot[:, :1]
        var = tot[:, LANES // 2 : LANES // 2 + 1] - mean * mean
        inv = lax.rsqrt(var + EPS)
        normed = (conv[part] - mean) * inv
        pre = normed * gain[...] + shift[...]
        sig = sigmoid(pre)
        gp = gm[part] * sig * (1.0 + pre * (1.0 - sig))
        gn = gp * gain[...]
        conv[part] = normed
        gm[part] = gn
        gx = gn * normed
        st2[part] = jnp.where(
            lanes,
            jnp.sum(fold(gn), 1, keepdims=True),
            jnp.sum(fold(gx), 1, keepdims=True),
        )
        inv_s[part] = jnp.broadcast_to(inv, (ALIGN, LANES))

        @pl.when((i >= edge // ALIGN) & (i < (rows + edge) // ALIGN))
        def _():
            gpn = gp * normed
            colg[...] += gpn[:8] + gpn[8:]
            cols[...] += gp[:8] + gp[8:]

        return carry

    lax.fori_loop(0, mid // ALIGN, norm_step, 0)
    swap2 = remote(st2, st2_in, tp_send.at[1], tp_recv.at[1], (sp, 1 - tp))
    swap2.start()

    rg = jnp.sum(colg[...], 0, keepdims=True)
    rsh = jnp.sum(cols[...], 0, keepdims=True)
    groups = channels // LANES
    for k in range(groups):
        gs[sp, pl.ds(k, 1), :] = rg[:, k * LANES : (k + 1) * LANES]
        gs[sp, pl.ds(groups + k, 1), :] = rsh[:, k * LANES : (k + 1) * LANES]

    def send_gs(d, carry):
        remote(gs.at[sp], gs.at[sp], all_send.at[0], all_recv.at[0], (peer(d), tp)).start()
        return carry

    lax.fori_loop(1, n, send_gs, 0)
    swap2.wait_recv()

    def gc_step(i, carry):
        part = pl.ds(pl.multiple_of(i * ALIGN, ALIGN), ALIGN)
        tot = (st2[part] + st2_in[part]) * (1.0 / width)
        m1 = tot[:, :1]
        m2 = tot[:, LANES // 2 : LANES // 2 + 1]
        inv = inv_s[part][:, :1]
        gcw[part] = (inv * (gm[part] - m1 - conv[part] * m2)).astype(BF16)
        return carry

    lax.fori_loop(0, mid // ALIGN, gc_step, 0)

    @pl.when(sp == 0)
    def _():
        gcw[pl.ds(0, edge)] = jnp.zeros((edge, channels), BF16)

    @pl.when(sp == n - 1)
    def _():
        gcw[pl.ds(rows + edge, edge)] = jnp.zeros((edge, channels), BF16)

    if n * per > tiles:
        rs_src[pl.ds(tiles, n * per - tiles)] = jnp.zeros(
            (n * per - tiles, ALIGN, LANES), BF16
        )

    def spec_step(c, carry):
        dr = jnp.zeros((freqs, CHUNK), F32)
        di = jnp.zeros((freqs, CHUNK), F32)
        for b in range(2):
            spec = dot(mats[pl.ds(0, size)], gcw[pl.ds(b * plan.bwd_step, size), cut(c)])
            gs_spec[pl.ds(b * size, size), cut(c)] = spec
            re, im = spec[:freqs], spec[freqs:]
            hr = hs[pl.ds(b * size, freqs), cut(c)]
            hi = hs[pl.ds(b * size + freqs, freqs), cut(c)]
            dr = dr + hr * re + hi * im
            di = di + hr * im - hi * re
        prod = jnp.concatenate([dr, di], 0).astype(BF16)
        out = dot(mats[pl.ds(plan.at_lags, plan.tap_rows)], prod) * plan.lag_scale
        out = out.astype(BF16)
        for r in range(plan.tap_rows // ALIGN):
            for k in range(CHUNK // LANES):
                rs_src[r * groups + c * (CHUNK // LANES) + k] = out[
                    r * ALIGN : (r + 1) * ALIGN, k * LANES : (k + 1) * LANES
                ]
        return carry

    lax.fori_loop(0, chunks, spec_step, 0)

    def send_rs(d, carry):
        to = peer(d)
        remote(rs_src.at[pl.ds(to * per, per)], rs_in.at[sp],
               all_send.at[1], all_recv.at[1], (to, tp)).start()
        return carry

    lax.fori_loop(1, n, send_rs, 0)
    rs_in[sp] = rs_src[pl.ds(sp * per, per)]

    def out_step(c, carry):
        ta = ts[pl.ds(0, freqs), cut(c)]
        tb = ts[pl.ds(freqs, freqs), cut(c)]
        for b in range(2):
            re = gs_spec[pl.ds(b * size, freqs), cut(c)]
            im = gs_spec[pl.ds(b * size + freqs, freqs), cut(c)]
            prod = jnp.concatenate([re * ta - im * tb, -(re * tb + im * ta)], 0).astype(BF16)
            out = dot(mats[pl.ds(plan.at_grad + b * plan.bwd_out, plan.bwd_out)], prod)
            place = pl.ds(b * plan.bwd_out, plan.bwd_out)
            sig = sig_s[place, cut(c)]
            left = out * sig
            dv[place, cut(c)] = left.astype(BF16)
            dg[place, cut(c)] = (
                left * value[place, cut(c)].astype(F32) * (1.0 - sig)
            ).astype(BF16)
        return carry

    lax.fori_loop(0, chunks, out_step, 0)
    outs = [
        pltpu.make_async_copy(dv, dv_h, out_sem.at[0]),
        pltpu.make_async_copy(dg, dg_h, out_sem.at[1]),
    ]
    for out in outs:
        out.start()

    def settle(ref, k):
        part = ref.at[pl.ds(0, n - 1)]
        pltpu.make_async_copy(part, part, all_recv.at[k]).wait()

    def settle_sent(ref, k):
        part = ref.at[pl.ds(0, n - 1)]
        pltpu.make_async_copy(part, part, all_send.at[k]).wait()

    settle(rs_in, 1)
    zero = jnp.zeros((per, ALIGN, LANES), F32)
    summed = lax.fori_loop(0, n, lambda i, t: t + rs_in[i].astype(F32), zero)
    ag[sp] = summed.astype(BF16)

    def send_ag(d, carry):
        remote(ag.at[sp], ag.at[sp], all_send.at[2], all_recv.at[2], (peer(d), tp)).start()
        return carry

    lax.fori_loop(1, n, send_ag, 0)

    settle(gs, 0)
    small = lax.fori_loop(
        0, n, lambda i, t: t + gs[i], jnp.zeros(gs.shape[1:], F32)
    )
    dgs_o[...] = small * (1.0 / math.sqrt(total))

    for halo in halos:
        halo.wait_send()
    swap1.wait_send()
    swap2.wait_send()
    settle_sent(gs, 0)
    settle_sent(rs_in, 1)
    settle(ag, 2)
    for t in range(tiles):
        r, k = t // groups, t % groups
        count = min(ALIGN, plan.kernel - r * ALIGN)
        dt_o[pl.ds(r * ALIGN, count), pl.ds(k * LANES, LANES)] = ag[t // per, t % per].astype(F32)[
            :count
        ]
    settle_sent(ag, 2)
    for out in outs:
        out.wait()


def shards(n, value_in, gate_in, taps, gain, shift, w_out, grad_out):
    rows, channels = value_in.shape
    kernel = taps.shape[0]
    total = rows * n
    plan = Plan(rows, kernel, total)
    groups = channels // LANES
    tiles = plan.tap_rows // ALIGN * groups
    per = -(-tiles // n)
    model = grad_out.shape[1]
    mats = jnp.asarray(plan.mats, BF16)
    own = jnp.asarray(plan.own, BF16)
    ft = jnp.asarray(plan.taps, F32)
    hbm = pl.BlockSpec(memory_space=pl.ANY)
    vmem = pl.BlockSpec(memory_space=pltpu.VMEM)
    size, mid = plan.size, plan.mid
    chunks = channels // CHUNK
    dma = pltpu.SemaphoreType.DMA
    d_value, d_gate, d_taps, d_small = pl.pallas_call(
        functools.partial(body, plan, n, tiles, per, total),
        out_shape=(
            jax.ShapeDtypeStruct((rows, channels), BF16),
            jax.ShapeDtypeStruct((rows, channels), BF16),
            jax.ShapeDtypeStruct((kernel, channels), F32),
            jax.ShapeDtypeStruct((2 * groups, LANES), F32),
        ),
        in_specs=[hbm] * 10,
        out_specs=(hbm, hbm, vmem, vmem),
        scratch_shapes=[
            pltpu.VMEM((rows, channels), BF16),
            pltpu.VMEM((rows, channels), BF16),
            pltpu.VMEM((kernel, channels), F32),
            pltpu.VMEM((1, channels), F32),
            pltpu.VMEM((1, channels), F32),
            pltpu.VMEM((channels, model), BF16),
            pltpu.VMEM((mid, model), BF16),
            pltpu.VMEM(plan.mats.shape, BF16),
            pltpu.VMEM(plan.own.shape, BF16),
            pltpu.VMEM(plan.taps.shape, F32),
            pltpu.VMEM((rows, channels), F32),
            pltpu.VMEM((plan.wide, channels), BF16),
            pltpu.VMEM((mid, channels), F32),
            pltpu.VMEM((mid, channels), F32),
            pltpu.VMEM((mid, channels), BF16),
            pltpu.VMEM((size, channels), F32),
            pltpu.VMEM((2 * size, channels), F32),
            pltpu.VMEM((2 * size, channels), F32),
            pltpu.VMEM((mid, LANES), F32),
            pltpu.VMEM((mid, LANES), F32),
            pltpu.VMEM((mid, LANES), F32),
            pltpu.VMEM((mid, LANES), F32),
            pltpu.VMEM((mid, LANES), F32),
            pltpu.VMEM((mid, LANES), F32),
            pltpu.VMEM((mid, LANES), F32),
            pltpu.VMEM((8, channels), F32),
            pltpu.VMEM((8, channels), F32),
            pltpu.VMEM((n, 2 * groups, LANES), F32),
            pltpu.VMEM((n * per, ALIGN, LANES), BF16),
            pltpu.VMEM((n, per, ALIGN, LANES), BF16),
            pltpu.VMEM((n, per, ALIGN, LANES), BF16),
            pltpu.VMEM((rows, channels), BF16),
            pltpu.VMEM((rows, channels), BF16),
            dma((9,)), dma((chunks,)), dma((2,)), dma((4,)), dma((4,)),
            dma((2,)), dma((2,)), dma((3,)), dma((3,)),
        ],
        compiler_params=pltpu.CompilerParams(
            collective_id=0, has_side_effects=True, vmem_limit_bytes=48 * 1024 * 1024
        ),
    )(
        value_in, gate_in, taps, gain.reshape(1, -1), shift.reshape(1, -1), w_out,
        grad_out, mats, own, ft,
    )
    flat = d_small.reshape(2, channels)
    return (d_value, d_gate, d_taps, flat[0], flat[1])


def solution(mesh):
    return jax.shard_map(
        functools.partial(shards, mesh.shape["sp"]),
        mesh=mesh,
        in_specs=(
            P("sp", "tp"),
            P("sp", "tp"),
            P(None, "tp"),
            P("tp"),
            P("tp"),
            P("tp", None),
            P("sp", None),
        ),
        out_specs=(P("sp", "tp"), P("sp", "tp"), P(None, "tp"), P("tp"), P("tp")),
        check_vma=False,
    )
```

time: 176 us -> 47.4 us (0.27)
  waiting for transfers between devices: 106 us -> 0 us
  Pallas kernels: 0 us -> 35.1 us
  other arithmetic: 24.5 us -> 0 us
  between operations: 14.5 us -> 0.66 us
  starting transfers between devices: 12.4 us -> 0 us
  matrix products: 5.53 us -> 0 us
  blocking collectives: 4.91 us -> 0 us
  local copies, waits for them, and re-layouts: 7.63 us -> 11.2 us
    psum x1 -> x0, waiting for transfers between devices: 101 us -> none  [shards(): summed = lax.psum(stacked, 'sp')]
    pallas_call x0 -> x1, Pallas kernels: none -> 35.1 us  [shards(): pl.pallas_call(functools.partial(body, plan, n, tiles, per, total), out_s...]
    reduce_sum x3 -> x0, other arithmetic: 12.9 us -> none  [the longest x2 7.23 us: shards(): jnp.sum(own_grad * gated_float[offset:offset + rows], 0)]
    ppermute x4 -> x0, starting transfers between devices: 12.4 us -> none  [the longest x2 9.8 us: with_halo(): lax.ppermute(lax.slice_in_dim(block, block.shape[dim] - width, None, axis...]
    convert_element_type x4 -> x0, other arithmetic: 10.9 us -> none  [the longest x1 6.89 us: shards(): (grad_gated * value_in.astype(jnp.float32) * gate_sig * (1.0 - gate_sig))...]
    unnamed x52 -> x21, local copies, waits for them, and re-layouts: 0.12 us -> 10.6 us
    dot_general x1 -> x0, matrix products: 5.53 us -> none  [norm_backward(): lax.dot_general(grad_rows, w_out, (((1,), (1,)), ((), ())), preferred_ele...]
    psum x2 -> x0, blocking collectives: 4.91 us -> none  [the longest x1 2.47 us: norm_backward(): lax.psum((jnp.sum(conv_out, 1), jnp.sum(conv_out * conv_out, 1)), 'tp')]
  transfers between devices with their start and end apart: 5 -> 0, of which waited for: 2 -> 0; matrix products, arithmetic and copies ran while one was open for 8% -> 0% of each run, Pallas kernels for 0% -> 0%
where the time goes in v1:
time: 47.4 us; the launch traced here: 47 us
  Pallas kernels  35.1 us (74%)
  local copies, waits for them, and re-layouts  11.2 us (24%)
  between operations  0.66 us (1%)
    pallas_call x1, Pallas kernels, shards(): pl.pallas_call(functools.partial(body, plan, n, tiles, per, total), out_s...  35.1 us
    unnamed x21, local copies, waits for them, and re-layouts  10.6 us

profile of v1, /device:TPU:0, one launch (start us, length us, event | category | flops | bytes accessed | tf_op | source)
XLA Modules:
  0.0 47.0 jit_solution(8262770060406974261)
XLA Ops:
  0.6 0.0 copy-start
  0.6 1.2 %copy-done = bf16[256,2048]{1,0:T(8,128)(2,1)S(1)} copy-done((bf16[256,2048]{1,0:T(8,128)(2,1)S(1)}, bf16[256,2048]{1,0:T(8,128)(2,1)}, u32[]{:S(2)}) %copy-start) | copy-done | bytes 1048600
  1.9 0.0 copy-start.1
  1.9 1.0 %copy-done.1 = bf16[256,1024]{1,0:T(8,128)(2,1)S(1)} copy-done((bf16[256,1024]{1,0:T(8,128)(2,1)S(1)}, bf16[256,1024]{1,0:T(8,128)(2,1)}, u32[]{:S(2)}) %copy-start.1) | copy-done | bytes 524312
  2.9 0.0 copy-start.2
  2.9 1.0 %copy-done.2 = bf16[256,1024]{1,0:T(8,128)(2,1)S(1)} copy-done((bf16[256,1024]{1,0:T(8,128)(2,1)S(1)}, bf16[256,1024]{1,0:T(8,128)(2,1)}, u32[]{:S(2)}) %copy-start.2) | copy-done | bytes 524312
  3.9 0.0 copy-start.3
  3.9 1.0 %copy-done.3 = bf16[768,192]{1,0:T(8,128)(2,1)S(1)} copy-done((bf16[768,192]{1,0:T(8,128)(2,1)S(1)}, bf16[768,192]{1,0:T(8,128)(2,1)}, u32[]{:S(2)}) %copy-start.3) | copy-done | bytes 294936
  4.9 0.0 copy-start.4
  4.9 0.9 %copy-done.4 = f32[31,1024]{1,0:T(8,128)S(1)} copy-done((f32[31,1024]{1,0:T(8,128)S(1)}, f32[31,1024]{1,0:T(8,128)}, u32[]{:S(2)}) %copy-start.4) | copy-done | bytes 127000
  5.8 0.0 copy-start.5
  5.8 0.9 %copy-done.5 = f32[192,31]{1,0:T(8,128)S(1)} copy-done((f32[192,31]{1,0:T(8,128)S(1)}, f32[192,31]{1,0:T(8,128)}, u32[]{:S(2)}) %copy-start.5) | copy-done | bytes 23832
  6.7 0.0 copy-start.6
  6.7 0.9 %copy-done.6 = bf16[384,128]{1,0:T(8,128)(2,1)S(1)} copy-done((bf16[384,128]{1,0:T(8,128)(2,1)S(1)}, bf16[384,128]{1,0:T(8,128)(2,1)}, u32[]{:S(2)}) %copy-start.6) | copy-done | bytes 98328
  7.6 0.0 copy-start.7
  7.6 0.7 %copy-done.7 = f32[1024]{0:T(1024)S(1)} copy-done((f32[1024]{0:T(1024)S(1)}, f32[1024]{0:T(1024)}, u32[]{:S(2)}) %copy-start.7) | copy-done | bytes 4120
  8.3 0.0 copy-start.8
  8.3 0.7 %copy-done.8 = f32[1024]{0:T(1024)S(1)} copy-done((f32[1024]{0:T(1024)S(1)}, f32[1024]{0:T(1024)}, u32[]{:S(2)}) %copy-start.8) | copy-done | bytes 4120
  9.0 35.1 %shard_map.137 = (bf16[256,1024]{1,0:T(8,128)(2,1)S(1)}, bf16[256,1024]{1,0:T(8,128)(2,1)S(1)}, f32[31,1024]{1,0:T(8,128)S(1)}, f32[16,128]{1,0:T(8,128)S(1)}) custom-call(bf16[256,1024]{1,0:T(8,128)(2,1)S(1)} %copy-done.1, bf16[256,1024]{1,0:T(8,128)(2,1)S(1)} %copy-done.2, f32[31,1024]{1,0:T(8,128)S(1)} %copy-done.4, f32[1,1024]{1,0:T(1,128)S(1)} %bitcast.6, ...), custom_call_target="tpu_custom_call" | custom-call | tf_op jit(solution)/shard_map/pallas_call | solution.py:451
  44.1 0.6 %slice_bitcast_fusion = (f32[1024]{0:T(1024)}, f32[1024]{0:T(1024)}) fusion(f32[16,128]{1,0:T(8,128)S(1)} %get-tuple-element.12), kind=kLoop, calls=%fused_computation | loop fusion | bytes 16384 | tf_op jit(solution)/shard_map/squeeze | solution.py:506
  44.7 0.8 %copy.18 = bf16[256,1024]{1,0:T(8,128)(2,1)} copy(bf16[256,1024]{1,0:T(8,128)(2,1)S(1)} %get-tuple-element.20) | data formatting | bytes 1048576
  45.5 0.8 %copy.19 = bf16[256,1024]{1,0:T(8,128)(2,1)} copy(bf16[256,1024]{1,0:T(8,128)(2,1)S(1)} %get-tuple-element.21) | data formatting | bytes 1048576
  46.3 0.7 %copy.20 = f32[31,1024]{1,0:T(8,128)} copy(f32[31,1024]{1,0:T(8,128)S(1)} %get-tuple-element.22) | data formatting | bytes 253952
Async XLA Ops:
  0.6 1.2 %copy-start = (bf16[256,2048]{1,0:T(8,128)(2,1)S(1)}, bf16[256,2048]{1,0:T(8,128)(2,1)}, u32[]{:S(2)}) copy-start(bf16[256,2048]{1,0:T(8,128)(2,1)} %go_h.1) | copy-start | bytes 3145732
  1.9 1.0 %copy-start.1 = (bf16[256,1024]{1,0:T(8,128)(2,1)S(1)}, bf16[256,1024]{1,0:T(8,128)(2,1)}, u32[]{:S(2)}) copy-start(bf16[256,1024]{1,0:T(8,128)(2,1)} %value_h.1) | copy-start | bytes 1572868
  2.9 1.0 %copy-start.2 = (bf16[256,1024]{1,0:T(8,128)(2,1)S(1)}, bf16[256,1024]{1,0:T(8,128)(2,1)}, u32[]{:S(2)}) copy-start(bf16[256,1024]{1,0:T(8,128)(2,1)} %gate_h.1) | copy-start | bytes 1572868
  3.9 1.0 %copy-start.3 = (bf16[768,192]{1,0:T(8,128)(2,1)S(1)}, bf16[768,192]{1,0:T(8,128)(2,1)}, u32[]{:S(2)}) copy-start(bf16[768,192]{1,0:T(8,128)(2,1)} %constant.6.clone.mats_h) | copy-start | bytes 884740
  4.9 0.9 %copy-start.4 = (f32[31,1024]{1,0:T(8,128)S(1)}, f32[31,1024]{1,0:T(8,128)}, u32[]{:S(2)}) copy-start(f32[31,1024]{1,0:T(8,128)} %taps_h.1) | copy-start | bytes 380932
  5.8 0.9 %copy-start.5 = (f32[192,31]{1,0:T(8,128)S(1)}, f32[192,31]{1,0:T(8,128)}, u32[]{:S(2)}) copy-start(f32[192,31]{1,0:T(8,128)} %constant.8.clone.ft_h) | copy-start | bytes 71428
  6.7 0.9 %copy-start.6 = (bf16[384,128]{1,0:T(8,128)(2,1)S(1)}, bf16[384,128]{1,0:T(8,128)(2,1)}, u32[]{:S(2)}) copy-start(bf16[384,128]{1,0:T(8,128)(2,1)} %constant.7.clone.own_h) | copy-start | bytes 294916
  7.6 0.7 %copy-start.7 = (f32[1024]{0:T(1024)S(1)}, f32[1024]{0:T(1024)}, u32[]{:S(2)}) copy-start(f32[1024]{0:T(1024)} %param.13) | copy-start | bytes 12292
  8.3 0.7 %copy-start.8 = (f32[1024]{0:T(1024)S(1)}, f32[1024]{0:T(1024)}, u32[]{:S(2)}) copy-start(f32[1024]{0:T(1024)} %param.14) | copy-start | bytes 12292

commit v2 on v1

--- a/solution.py
+++ b/solution.py
@@ -77,12 +77,12 @@
 def body(
     plan, n, tiles, per, total,
     value_h, gate_h, taps_h, gain_h, shift_h, w_h, go_h, mats_h, own_h, ft_h,
-    dv_h, dg_h, dt_o, dgs_o,
+    dv, dg, dt_o, dgs_o,
     value, gate, taps, gain, shift, w, go, mats, own, ft,
     sig_s, gw, conv, gm, gcw, ts, hs, gs_spec, acc1, acc2,
     st1, st1_in, st2, st2_in, inv_s, colg, cols,
-    gs, rs_src, rs_in, ag, dv, dg,
-    load_sem, w_sem, out_sem, halo_send, halo_recv, tp_send, tp_recv,
+    gs, rs_src, rs_in, ag,
+    load_sem, w_sem, halo_send, halo_recv, tp_send, tp_recv,
     all_send, all_recv,
 ):
     sp = lax.axis_index("sp")
@@ -381,13 +381,6 @@
         return carry
 
     lax.fori_loop(0, chunks, out_step, 0)
-    outs = [
-        pltpu.make_async_copy(dv, dv_h, out_sem.at[0]),
-        pltpu.make_async_copy(dg, dg_h, out_sem.at[1]),
-    ]
-    for out in outs:
-        out.start()
-
     def settle(ref, k):
         part = ref.at[pl.ds(0, n - 1)]
         pltpu.make_async_copy(part, part, all_recv.at[k]).wait()
@@ -427,8 +420,21 @@
             :count
         ]
     settle_sent(ag, 2)
-    for out in outs:
-        out.wait()
+
+
+def store(parts, *refs):
+    sources, targets, sem = refs[:parts], refs[parts:-1], refs[-1]
+    groups = sources[-1].shape[0] // 2
+    views = list(sources[:-1]) + [
+        sources[-1].at[pl.ds(0, groups)], sources[-1].at[pl.ds(groups, groups)]
+    ]
+    copies = [
+        pltpu.make_async_copy(a, b, sem.at[i]) for i, (a, b) in enumerate(zip(views, targets))
+    ]
+    for copy in copies:
+        copy.start()
+    for copy in copies:
+        copy.wait()
 
 
 def shards(n, value_in, gate_in, taps, gain, shift, w_out, grad_out):
@@ -443,12 +449,12 @@
     mats = jnp.asarray(plan.mats, BF16)
     own = jnp.asarray(plan.own, BF16)
     ft = jnp.asarray(plan.taps, F32)
-    hbm = pl.BlockSpec(memory_space=pl.ANY)
+    hbm = pl.BlockSpec(memory_space=pltpu.HBM)
     vmem = pl.BlockSpec(memory_space=pltpu.VMEM)
     size, mid = plan.size, plan.mid
     chunks = channels // CHUNK
     dma = pltpu.SemaphoreType.DMA
-    d_value, d_gate, d_taps, d_small = pl.pallas_call(
+    results = pl.pallas_call(
         functools.partial(body, plan, n, tiles, per, total),
         out_shape=(
             jax.ShapeDtypeStruct((rows, channels), BF16),
@@ -457,7 +463,7 @@
             jax.ShapeDtypeStruct((2 * groups, LANES), F32),
         ),
         in_specs=[hbm] * 10,
-        out_specs=(hbm, hbm, vmem, vmem),
+        out_specs=(vmem,) * 4,
         scratch_shapes=[
             pltpu.VMEM((rows, channels), BF16),
             pltpu.VMEM((rows, channels), BF16),
@@ -490,9 +496,7 @@
             pltpu.VMEM((n * per, ALIGN, LANES), BF16),
             pltpu.VMEM((n, per, ALIGN, LANES), BF16),
             pltpu.VMEM((n, per, ALIGN, LANES), BF16),
-            pltpu.VMEM((rows, channels), BF16),
-            pltpu.VMEM((rows, channels), BF16),
-            dma((9,)), dma((chunks,)), dma((2,)), dma((4,)), dma((4,)),
+            dma((9,)), dma((chunks,)), dma((4,)), dma((4,)),
             dma((2,)), dma((2,)), dma((3,)), dma((3,)),
         ],
         compiler_params=pltpu.CompilerParams(
@@ -502,8 +506,20 @@
         value_in, gate_in, taps, gain.reshape(1, -1), shift.reshape(1, -1), w_out,
         grad_out, mats, own, ft,
     )
-    flat = d_small.reshape(2, channels)
-    return (d_value, d_gate, d_taps, flat[0], flat[1])
+    d_value, d_gate, d_taps, d_gain, d_shift = pl.pallas_call(
+        functools.partial(store, 4),
+        out_shape=(
+            jax.ShapeDtypeStruct((rows, channels), BF16),
+            jax.ShapeDtypeStruct((rows, channels), BF16),
+            jax.ShapeDtypeStruct((kernel, channels), F32),
+            jax.ShapeDtypeStruct((groups, LANES), F32),
+            jax.ShapeDtypeStruct((groups, LANES), F32),
+        ),
+        in_specs=[vmem] * 4,
+        out_specs=(hbm,) * 5,
+        scratch_shapes=[dma((5,))],
+    )(*results)
+    return (d_value, d_gate, d_taps, d_gain.reshape(-1), d_shift.reshape(-1))
 
 
 def solution(mesh):

time: 47.4 us -> 49.6 us (1.046)
  Pallas kernels: 35.1 us -> 37.3 us
    pallas_call x0 -> x1, Pallas kernels: none -> 2.27 us  [shards(): pl.pallas_call(functools.partial(store, 4), out_shape=(jax.ShapeDtypeStru...]
    squeeze x1 -> x0, local copies, waits for them, and re-layouts: 0.6 us -> none  [shards(): return (d_value, d_gate, d_taps, flat[0], flat[1])]
    unnamed x21 -> x26, local copies, waits for them, and re-layouts: 10.6 us -> 11.2 us
where the time goes in v2:
time: 49.6 us; the launch traced here: 49.2 us
  Pallas kernels  37.3 us (75%)
  local copies, waits for them, and re-layouts  11.2 us (23%)
  between operations  0.67 us (1%)
    pallas_call x1, Pallas kernels, shards(): pl.pallas_call(functools.partial(body, plan, n, tiles, per, total), out_s...  35.1 us
    unnamed x26, local copies, waits for them, and re-layouts  11.2 us
    pallas_call x1, Pallas kernels, shards(): pl.pallas_call(functools.partial(store, 4), out_shape=(jax.ShapeDtypeStru...  2.27 us

profile of v2, /device:TPU:0, one launch (start us, length us, event | category | flops | bytes accessed | tf_op | source)
XLA Modules:
  0.0 49.2 jit_solution(4496689804046555573)
XLA Ops:
  0.6 0.0 copy-start
  0.6 1.2 %copy-done = bf16[256,2048]{1,0:T(8,128)(2,1)S(1)} copy-done((bf16[256,2048]{1,0:T(8,128)(2,1)S(1)}, bf16[256,2048]{1,0:T(8,128)(2,1)}, u32[]{:S(2)}) %copy-start) | copy-done | bytes 1048600
  1.9 0.0 copy-start.3
  1.9 1.0 %copy-done.3 = bf16[256,1024]{1,0:T(8,128)(2,1)S(1)} copy-done((bf16[256,1024]{1,0:T(8,128)(2,1)S(1)}, bf16[256,1024]{1,0:T(8,128)(2,1)}, u32[]{:S(2)}) %copy-start.3) | copy-done | bytes 524312
  2.9 0.0 copy-start.4
  2.9 1.0 %copy-done.4 = bf16[256,1024]{1,0:T(8,128)(2,1)S(1)} copy-done((bf16[256,1024]{1,0:T(8,128)(2,1)S(1)}, bf16[256,1024]{1,0:T(8,128)(2,1)}, u32[]{:S(2)}) %copy-start.4) | copy-done | bytes 524312
  3.9 0.0 copy-start.5
  3.9 1.0 %copy-done.5 = bf16[768,192]{1,0:T(8,128)(2,1)S(1)} copy-done((bf16[768,192]{1,0:T(8,128)(2,1)S(1)}, bf16[768,192]{1,0:T(8,128)(2,1)}, u32[]{:S(2)}) %copy-start.5) | copy-done | bytes 294936
  4.9 0.0 copy-start.6
  4.9 0.9 %copy-done.6 = f32[31,1024]{1,0:T(8,128)S(1)} copy-done((f32[31,1024]{1,0:T(8,128)S(1)}, f32[31,1024]{1,0:T(8,128)}, u32[]{:S(2)}) %copy-start.6) | copy-done | bytes 127000
  5.8 0.0 copy-start.8
  5.8 0.9 %copy-done.8 = f32[192,31]{1,0:T(8,128)S(1)} copy-done((f32[192,31]{1,0:T(8,128)S(1)}, f32[192,31]{1,0:T(8,128)}, u32[]{:S(2)}) %copy-start.8) | copy-done | bytes 23832
  6.7 0.0 copy-start.9
  6.7 0.9 %copy-done.9 = bf16[384,128]{1,0:T(8,128)(2,1)S(1)} copy-done((bf16[384,128]{1,0:T(8,128)(2,1)S(1)}, bf16[384,128]{1,0:T(8,128)(2,1)}, u32[]{:S(2)}) %copy-start.9) | copy-done | bytes 98328
  7.6 0.0 copy-start.11
  7.6 0.7 %copy-done.11 = f32[1024]{0:T(1024)S(1)} copy-done((f32[1024]{0:T(1024)S(1)}, f32[1024]{0:T(1024)}, u32[]{:S(2)}) %copy-start.11) | copy-done | bytes 4120
  8.3 0.0 copy-start.12
  8.3 0.7 %copy-done.12 = f32[1024]{0:T(1024)S(1)} copy-done((f32[1024]{0:T(1024)S(1)}, f32[1024]{0:T(1024)}, u32[]{:S(2)}) %copy-start.12) | copy-done | bytes 4120
  9.0 35.1 %shard_map.137 = (bf16[256,1024]{1,0:T(8,128)(2,1)S(1)}, bf16[256,1024]{1,0:T(8,128)(2,1)S(1)}, f32[31,1024]{1,0:T(8,128)S(1)}, f32[16,128]{1,0:T(8,128)S(1)}) custom-call(bf16[256,1024]{1,0:T(8,128)(2,1)S(1)} %copy-done.3, bf16[256,1024]{1,0:T(8,128)(2,1)S(1)} %copy-done.4, f32[31,1024]{1,0:T(8,128)S(1)} %copy-done.6, f32[1,1024]{1,0:T(1,128)S(1)} %bitcast.4, ...), custom_call_target="tpu_custom_call" | custom-call | tf_op jit(solution)/shard_map/pallas_call | solution.py:457
  44.1 0.0 copy-start.1
  44.1 0.8 %copy-done.1 = bf16[256,1024]{1,0:T(8,128)(2,1)} copy-done((bf16[256,1024]{1,0:T(8,128)(2,1)}, bf16[256,1024]{1,0:T(8,128)(2,1)S(1)}, u32[]{:S(2)}) %copy-start.1) | copy-done | bytes 524312
  44.9 0.0 copy-start.2
  44.9 0.8 %copy-done.2 = bf16[256,1024]{1,0:T(8,128)(2,1)} copy-done((bf16[256,1024]{1,0:T(8,128)(2,1)}, bf16[256,1024]{1,0:T(8,128)(2,1)S(1)}, u32[]{:S(2)}) %copy-start.2) | copy-done | bytes 524312
  45.7 0.0 copy-start.7
  45.7 0.6 %copy-done.7 = f32[31,1024]{1,0:T(8,128)} copy-done((f32[31,1024]{1,0:T(8,128)}, f32[31,1024]{1,0:T(8,128)S(1)}, u32[]{:S(2)}) %copy-start.7) | copy-done | bytes 127000
  46.3 0.0 copy-start.10
  46.3 0.6 %copy-done.10 = f32[16,128]{1,0:T(8,128)} copy-done((f32[16,128]{1,0:T(8,128)}, f32[16,128]{1,0:T(8,128)S(1)}, u32[]{:S(2)}) %copy-start.10) | copy-done | bytes 8216
  46.9 2.3 %shard_map.138 = (bf16[256,1024]{1,0:T(8,128)(2,1)}, bf16[256,1024]{1,0:T(8,128)(2,1)}, f32[31,1024]{1,0:T(8,128)}, f32[8,128]{1,0:T(8,128)}, f32[8,128]{1,0:T(8,128)}) custom-call(bf16[256,1024]{1,0:T(8,128)(2,1)} %copy-done.1, bf16[256,1024]{1,0:T(8,128)(2,1)} %copy-done.2, f32[31,1024]{1,0:T(8,128)} %copy-done.7, f32[16,128]{1,0:T(8,128)} %copy-done.10), custom_call_target="tpu_custom_call" | custom-call | tf_op jit(solution)/shard_map/pallas_call | solution.py:509
Async XLA Ops:
  0.6 1.2 %copy-start = (bf16[256,2048]{1,0:T(8,128)(2,1)S(1)}, bf16[256,2048]{1,0:T(8,128)(2,1)}, u32[]{:S(2)}) copy-start(bf16[256,2048]{1,0:T(8,128)(2,1)} %go_h.1) | copy-start | bytes 3145732
  1.9 1.0 %copy-start.3 = (bf16[256,1024]{1,0:T(8,128)(2,1)S(1)}, bf16[256,1024]{1,0:T(8,128)(2,1)}, u32[]{:S(2)}) copy-start(bf16[256,1024]{1,0:T(8,128)(2,1)} %value_h.1) | copy-start | bytes 1572868
  2.9 1.0 %copy-start.4 = (bf16[256,1024]{1,0:T(8,128)(2,1)S(1)}, bf16[256,1024]{1,0:T(8,128)(2,1)}, u32[]{:S(2)}) copy-start(bf16[256,1024]{1,0:T(8,128)(2,1)} %gate_h.1) | copy-start | bytes 1572868
  3.9 1.0 %copy-start.5 = (bf16[768,192]{1,0:T(8,128)(2,1)S(1)}, bf16[768,192]{1,0:T(8,128)(2,1)}, u32[]{:S(2)}) copy-start(bf16[768,192]{1,0:T(8,128)(2,1)} %constant.6.clone.mats_h) | copy-start | bytes 884740
  4.9 0.9 %copy-start.6 = (f32[31,1024]{1,0:T(8,128)S(1)}, f32[31,1024]{1,0:T(8,128)}, u32[]{:S(2)}) copy-start(f32[31,1024]{1,0:T(8,128)} %taps_h.1) | copy-start | bytes 380932
  5.8 0.9 %copy-start.8 = (f32[192,31]{1,0:T(8,128)S(1)}, f32[192,31]{1,0:T(8,128)}, u32[]{:S(2)}) copy-start(f32[192,31]{1,0:T(8,128)} %constant.8.clone.ft_h) | copy-start | bytes 71428
  6.7 0.9 %copy-start.9 = (bf16[384,128]{1,0:T(8,128)(2,1)S(1)}, bf16[384,128]{1,0:T(8,128)(2,1)}, u32[]{:S(2)}) copy-start(bf16[384,128]{1,0:T(8,128)(2,1)} %constant.7.clone.own_h) | copy-start | bytes 294916
  7.6 0.7 %copy-start.11 = (f32[1024]{0:T(1024)S(1)}, f32[1024]{0:T(1024)}, u32[]{:S(2)}) copy-start(f32[1024]{0:T(1024)} %param.13) | copy-start | bytes 12292
  8.3 0.7 %copy-start.12 = (f32[1024]{0:T(1024)S(1)}, f32[1024]{0:T(1024)}, u32[]{:S(2)}) copy-start(f32[1024]{0:T(1024)} %param.14) | copy-start | bytes 12292
  44.1 0.8 %copy-start.1 = (bf16[256,1024]{1,0:T(8,128)(2,1)}, bf16[256,1024]{1,0:T(8,128)(2,1)S(1)}, u32[]{:S(2)}) copy-start(bf16[256,1024]{1,0:T(8,128)(2,1)S(1)} %get-tuple-element.14.refs_0_) | copy-start | bytes 1572868
  44.9 0.8 %copy-start.2 = (bf16[256,1024]{1,0:T(8,128)(2,1)}, bf16[256,1024]{1,0:T(8,128)(2,1)S(1)}, u32[]{:S(2)}) copy-start(bf16[256,1024]{1,0:T(8,128)(2,1)S(1)} %get-tuple-element.15.refs_1_) | copy-start | bytes 1572868
  45.7 0.7 %copy-start.7 = (f32[31,1024]{1,0:T(8,128)}, f32[31,1024]{1,0:T(8,128)S(1)}, u32[]{:S(2)}) copy-start(f32[31,1024]{1,0:T(8,128)S(1)} %get-tuple-element.16.refs_2_) | copy-start | bytes 380932
  46.3 0.6 %copy-start.10 = (f32[16,128]{1,0:T(8,128)}, f32[16,128]{1,0:T(8,128)S(1)}, u32[]{:S(2)}) copy-start(f32[16,128]{1,0:T(8,128)S(1)} %get-tuple-element.17.refs_3_) | copy-start | bytes 24580

commit v3 on v1

--- a/solution.py
+++ b/solution.py
@@ -13,6 +13,7 @@
 ALIGN = 16
 LANES = 128
 CHUNK = 256
+VMEM_GRANT = 62 * 1024 * 1024
 F32 = jnp.float32
 BF16 = jnp.bfloat16
 
@@ -431,6 +432,29 @@
         out.wait()
 
 
+def store(*refs):
+    sources, targets, holds = refs[:4], refs[4:9], refs[9:13]
+    in_sem, out_sem = refs[13:]
+    groups = holds[3].shape[0] // 2
+    views = list(holds[:3]) + [
+        holds[3].at[pl.ds(0, groups)], holds[3].at[pl.ds(groups, groups)]
+    ]
+    loads = [
+        pltpu.make_async_copy(a, b, in_sem.at[i]) for i, (a, b) in enumerate(zip(sources, holds))
+    ]
+    copies = [
+        pltpu.make_async_copy(a, b, out_sem.at[i]) for i, (a, b) in enumerate(zip(views, targets))
+    ]
+    for load in loads:
+        load.start()
+    for i, copy in enumerate(copies):
+        if i < len(loads):
+            loads[i].wait()
+        copy.start()
+    for copy in copies:
+        copy.wait()
+
+
 def shards(n, value_in, gate_in, taps, gain, shift, w_out, grad_out):
     rows, channels = value_in.shape
     kernel = taps.shape[0]
@@ -443,12 +467,12 @@
     mats = jnp.asarray(plan.mats, BF16)
     own = jnp.asarray(plan.own, BF16)
     ft = jnp.asarray(plan.taps, F32)
-    hbm = pl.BlockSpec(memory_space=pl.ANY)
+    hbm = pl.BlockSpec(memory_space=pltpu.HBM)
     vmem = pl.BlockSpec(memory_space=pltpu.VMEM)
     size, mid = plan.size, plan.mid
     chunks = channels // CHUNK
     dma = pltpu.SemaphoreType.DMA
-    d_value, d_gate, d_taps, d_small = pl.pallas_call(
+    results = pl.pallas_call(
         functools.partial(body, plan, n, tiles, per, total),
         out_shape=(
             jax.ShapeDtypeStruct((rows, channels), BF16),
@@ -496,14 +520,33 @@
             dma((2,)), dma((2,)), dma((3,)), dma((3,)),
         ],
         compiler_params=pltpu.CompilerParams(
-            collective_id=0, has_side_effects=True, vmem_limit_bytes=48 * 1024 * 1024
+            collective_id=0, has_side_effects=True, vmem_limit_bytes=VMEM_GRANT
         ),
     )(
         value_in, gate_in, taps, gain.reshape(1, -1), shift.reshape(1, -1), w_out,
         grad_out, mats, own, ft,
     )
-    flat = d_small.reshape(2, channels)
-    return (d_value, d_gate, d_taps, flat[0], flat[1])
+    d_value, d_gate, d_taps, d_gain, d_shift = pl.pallas_call(
+        store,
+        out_shape=(
+            jax.ShapeDtypeStruct((rows, channels), BF16),
+            jax.ShapeDtypeStruct((rows, channels), BF16),
+            jax.ShapeDtypeStruct((kernel, channels), F32),
+            jax.ShapeDtypeStruct((groups, LANES), F32),
+            jax.ShapeDtypeStruct((groups, LANES), F32),
+        ),
+        in_specs=[hbm] * 4,
+        out_specs=(hbm,) * 5,
+        scratch_shapes=[
+            pltpu.VMEM((rows, channels), BF16),
+            pltpu.VMEM((rows, channels), BF16),
+            pltpu.VMEM((kernel, channels), F32),
+            pltpu.VMEM((2 * groups, LANES), F32),
+            dma((4,)), dma((5,)),
+        ],
+        compiler_params=pltpu.CompilerParams(vmem_limit_bytes=VMEM_GRANT),
+    )(*results)
+    return (d_value, d_gate, d_taps, d_gain.reshape(-1), d_shift.reshape(-1))
 
 
 def solution(mesh):

time: 47.4 us -> 39.3 us (0.83)
  local copies, waits for them, and re-layouts: 11.2 us -> 0 us
  Pallas kernels: 35.1 us -> 38.5 us
    unnamed x21 -> x0, local copies, waits for them, and re-layouts: 10.6 us -> none
    pallas_call x0 -> x1, Pallas kernels: none -> 2.12 us  [shards(): pl.pallas_call(store, out_shape=(jax.ShapeDtypeStruct((rows, channels), B...]
    pallas_call x1, Pallas kernels: 35.1 us -> 36.4 us  [shards(): pl.pallas_call(functools.partial(body, plan, n, tiles, per, total), out_s...]
    squeeze x1 -> x0, local copies, waits for them, and re-layouts: 0.6 us -> none  [shards(): return (d_value, d_gate, d_taps, flat[0], flat[1])]
where the time goes in v3:
time: 39.3 us; the launch traced here: 39.2 us
  Pallas kernels  38.5 us (98%)
  between operations  0.64 us (2%)
    pallas_call x1, Pallas kernels, shards(): pl.pallas_call(functools.partial(body, plan, n, tiles, per, total), out_s...  36.4 us
    pallas_call x1, Pallas kernels, shards(): pl.pallas_call(store, out_shape=(jax.ShapeDtypeStruct((rows, channels), B...  2.12 us

profile of v3, /device:TPU:0, one launch (start us, length us, event | category | flops | bytes accessed | tf_op | source)
XLA Modules:
  0.0 39.2 jit_solution(15516306004220542185)
XLA Ops:
  0.6 36.4 %shard_map.137 = (bf16[256,1024]{1,0:T(8,128)(2,1)}, bf16[256,1024]{1,0:T(8,128)(2,1)}, f32[31,1024]{1,0:T(8,128)}, f32[16,128]{1,0:T(8,128)}) custom-call(bf16[256,1024]{1,0:T(8,128)(2,1)} %value_h.1, bf16[256,1024]{1,0:T(8,128)(2,1)} %gate_h.1, f32[31,1024]{1,0:T(8,128)} %taps_h.1, f32[1,1024]{1,0:T(1,128)} %bitcast.4, f32[1,1024]{1,0:T(1,128)} %bitcast.5, ...), custom_call_target="tpu_custom_call" | custom-call | tf_op jit(solution)/shard_map/pallas_call | solution.py:475
  37.1 2.1 %shard_map.138 = (bf16[256,1024]{1,0:T(8,128)(2,1)}, bf16[256,1024]{1,0:T(8,128)(2,1)}, f32[31,1024]{1,0:T(8,128)}, f32[8,128]{1,0:T(8,128)}, f32[8,128]{1,0:T(8,128)}) custom-call(bf16[256,1024]{1,0:T(8,128)(2,1)} %get-tuple-element.14.refs_0_, bf16[256,1024]{1,0:T(8,128)(2,1)} %get-tuple-element.15.refs_1_, f32[31,1024]{1,0:T(8,128)} %get-tuple-element.16.refs_2_, ...), custom_call_target="tpu_custom_call" | custom-call | tf_op jit(solution)/shard_map/pallas_call | solution.py:529

commit v4 on v3

--- a/solution.py
+++ b/solution.py
@@ -144,7 +144,7 @@
         gw[place] = (value[part].astype(F32) * sig).astype(BF16)
         return carry
 
-    lax.fori_loop(0, rows // ALIGN, gate_step, 0)
+    lax.fori_loop(0, rows // ALIGN, gate_step, 0, unroll=4)
     for load in loads[2:7]:
         load.wait()
 
@@ -155,7 +155,7 @@
         )
         return carry
 
-    lax.fori_loop(0, chunks, tap_step, 0)
+    lax.fori_loop(0, chunks, tap_step, 0, unroll=2)
 
     pl.semaphore_wait(barrier, n)
 
@@ -189,7 +189,7 @@
             )
         return carry
 
-    lax.fori_loop(0, chunks, own_step, 0)
+    lax.fori_loop(0, chunks, own_step, 0, unroll=2)
 
     def mix_step(c, carry):
         w_copy(c).wait()
@@ -232,7 +232,7 @@
             acc2[place] += fold(out * out)
         return carry
 
-    lax.fori_loop(0, chunks, conv_step, 0)
+    lax.fori_loop(0, chunks, conv_step, 0, unroll=2)
 
     first_lanes = lax.broadcasted_iota(jnp.int32, (mid, LANES), 1) < LANES // 2
     st1[...] = jnp.where(
@@ -282,15 +282,13 @@
         )
         inv_s[part] = jnp.broadcast_to(inv, (ALIGN, LANES))
 
-        @pl.when((i >= edge // ALIGN) & (i < (rows + edge) // ALIGN))
-        def _():
-            gpn = gp * normed
-            colg[...] += gpn[:8] + gpn[8:]
-            cols[...] += gp[:8] + gp[8:]
-
-        return carry
-
-    lax.fori_loop(0, mid // ALIGN, norm_step, 0)
+        inside = (i >= edge // ALIGN) & (i < (rows + edge) // ALIGN)
+        gpn = gp * normed
+        colg[...] += jnp.where(inside, gpn[:8] + gpn[8:], 0.0)
+        cols[...] += jnp.where(inside, gp[:8] + gp[8:], 0.0)
+        return carry
+
+    lax.fori_loop(0, mid // ALIGN, norm_step, 0, unroll=3)
     swap2 = remote(st2, st2_in, tp_send.at[1], tp_recv.at[1], (sp, 1 - tp))
     swap2.start()
 
@@ -317,7 +315,7 @@
         gcw[part] = (inv * (gm[part] - m1 - conv[part] * m2)).astype(BF16)
         return carry
 
-    lax.fori_loop(0, mid // ALIGN, gc_step, 0)
+    lax.fori_loop(0, mid // ALIGN, gc_step, 0, unroll=6)
 
     @pl.when(sp == 0)
     def _():
@@ -353,7 +351,7 @@
                 ]
         return carry
 
-    lax.fori_loop(0, chunks, spec_step, 0)
+    lax.fori_loop(0, chunks, spec_step, 0, unroll=2)
 
     def send_rs(d, carry):
         to = peer(d)
@@ -381,7 +379,7 @@
             ).astype(BF16)
         return carry
 
-    lax.fori_loop(0, chunks, out_step, 0)
+    lax.fori_loop(0, chunks, out_step, 0, unroll=2)
     outs = [
         pltpu.make_async_copy(dv, dv_h, out_sem.at[0]),
         pltpu.make_async_copy(dg, dg_h, out_sem.at[1]),

time: 39.3 us -> 34.9 us (0.89)
  Pallas kernels: 38.5 us -> 34.1 us
    pallas_call x1, Pallas kernels: 36.4 us -> 32 us  [shards(): pl.pallas_call(functools.partial(body, plan, n, tiles, per, total), out_s...]
where the time goes in v4:
time: 34.9 us; the launch traced here: 34.7 us
  Pallas kernels  34.1 us (98%)
  between operations  0.64 us (2%)
    pallas_call x1, Pallas kernels, shards(): pl.pallas_call(functools.partial(body, plan, n, tiles, per, total), out_s...  32 us
    pallas_call x1, Pallas kernels, shards(): pl.pallas_call(store, out_shape=(jax.ShapeDtypeStruct((rows, channels), B...  2.12 us

profile of v4, /device:TPU:0, one launch (start us, length us, event | category | flops | bytes accessed | tf_op | source)
XLA Modules:
  0.0 34.7 jit_solution(6893016497893283448)
XLA Ops:
  0.6 32.0 %shard_map.137 = (bf16[256,1024]{1,0:T(8,128)(2,1)}, bf16[256,1024]{1,0:T(8,128)(2,1)}, f32[31,1024]{1,0:T(8,128)}, f32[16,128]{1,0:T(8,128)}) custom-call(bf16[256,1024]{1,0:T(8,128)(2,1)} %value_h.1, bf16[256,1024]{1,0:T(8,128)(2,1)} %gate_h.1, f32[31,1024]{1,0:T(8,128)} %taps_h.1, f32[1,1024]{1,0:T(1,128)} %bitcast.4, f32[1,1024]{1,0:T(1,128)} %bitcast.5, ...), custom_call_target="tpu_custom_call" | custom-call | tf_op jit(solution)/shard_map/pallas_call | solution.py:473
  32.6 2.1 %shard_map.138 = (bf16[256,1024]{1,0:T(8,128)(2,1)}, bf16[256,1024]{1,0:T(8,128)(2,1)}, f32[31,1024]{1,0:T(8,128)}, f32[8,128]{1,0:T(8,128)}, f32[8,128]{1,0:T(8,128)}) custom-call(bf16[256,1024]{1,0:T(8,128)(2,1)} %get-tuple-element.14.refs_0_, bf16[256,1024]{1,0:T(8,128)(2,1)} %get-tuple-element.15.refs_1_, f32[31,1024]{1,0:T(8,128)} %get-tuple-element.16.refs_2_, ...), custom_call_target="tpu_custom_call" | custom-call | tf_op jit(solution)/shard_map/pallas_call | solution.py:527
